TPU v7x, 32 devices: a whole 2x2x4 slice. The times are simulated.
32 devices in a mesh: sp: 4 (over z), tp: 8 (over y, x, core).
Axes of the slice: x: 2, y: 2, z: 4, core: 2. Of those that a mesh axis runs over, the one named last changes fastest.
Arguments:
- context_activations: bfloat16 [2, 1024, 4096], P(None, 'sp', 'tp'), may hold values from -6 to 6
- first_generated_activation: bfloat16 [2, 4096], replicated, may hold values from -6 to 6
- address_projection: bfloat16 [4096, 1024], P(None, 'tp'), may hold values from -0.09375 to 0.09375
- payload_projection: bfloat16 [4096, 1024], P(None, 'tp'), may hold values from -0.09375 to 0.09375
- lookup_projection: bfloat16 [4096, 1024], P(None, 'tp'), may hold values from -0.09375 to 0.09375
- exit_gating_projection: bfloat16 [4096, 1024], P(None, 'tp'), may hold values from -0.09375 to 0.09375
- writing_intensity_projection: bfloat16 [4096, 8], replicated, may hold values from -0.09375 to 0.09375
- fading_projection: bfloat16 [4096, 8], replicated, may hold values from -0.09375 to 0.09375
- channel_fading_speed: float32 [8], replicated, may hold values from 0 to 1, as said below
- extra_fading_log: float32 [2, 1024, 8], P(None, 'sp', 'tp'), may hold values from -1 to 0, as said below
- readout_normalizer_gain: float32 [128], replicated, may hold values from 0.1 to 1.9
- exit_projection: bfloat16 [1024, 4096], P('tp'), may hold values from -0.1875 to 0.1875
Outputs:
- state_cache: bfloat16 [2, 4, 8, 128, 128], P(None, 'sp', 'tp')
- step_out: bfloat16 [2, 4096], P(None, 'tp')
Inputs may be any that keep to these rules, and one draw needn't show every extreme that they name: `channel_fading_speed`: positive rates, one a head. `extra_fading_log`: zero at all but a few positions of each prompt and head, negative there.
All inputs are finite; a program needn't handle non-finite values.
Results may differ from a plain program's by a relative error of at most 0.012.
Values may be sent and summed in bfloat16 or wider, within the bound.
A program may use at most 64 MiB of HBM per device.

v0:
```python
import jax
import jax.numpy as jnp
from jax import lax
from jax.sharding import PartitionSpec as P

BLOCK = 64
norm_eps = 1e-06
highest = lax.Precision.HIGHEST


def carried_in(value, axis, combine, identity):
    devices, position = (lax.axis_size(axis), lax.axis_index(axis))
    everything = jax.tree.map(
        lambda part, kind: lax.all_gather(part.astype(kind), axis),
        value,
        (jnp.bfloat16, jnp.bfloat16),
    )
    start = jax.tree.map(
        lambda part, zero: jnp.broadcast_to(jnp.asarray(zero, part.dtype), part.shape),
        value,
        identity,
    )

    def lap(k, before):
        reached = k < position
        new = combine(
            before, jax.tree.map(lambda part, own: part[k].astype(own.dtype), everything, value)
        )
        return jax.tree.map(lambda a, b: jnp.where(reached, a, b), new, before)

    return lax.fori_loop(0, devices, lap, start)


def carried_in_2(value, axis, combine, identity):
    devices, position = (lax.axis_size(axis), lax.axis_index(axis))
    everything = lax.all_gather(value, axis)
    start = jnp.broadcast_to(jnp.asarray(identity, value.dtype), value.shape)

    def lap(k, before):
        at = devices - 1 - k
        reached = at > position
        new = combine(before, everything[at])
        return jnp.where(reached, new, before)

    return lax.fori_loop(0, devices, lap, start)


def unit_rows(values_in):
    return values_in * lax.rsqrt(jnp.sum(values_in * values_in, axis=-1, keepdims=True) + norm_eps)


def compose(left, right):
    return jnp.einsum("...ij,...jk->...ik", left, right, precision=highest)


def segment_map(keys_in, values_in, beta_gate, fading_exponent):
    blocks = keys_in.shape[0] // BLOCK
    key_blocks = keys_in.reshape(blocks, BLOCK, -1)
    value_blocks = values_in.reshape(blocks, BLOCK, -1)
    beta_blocks = beta_gate.reshape(blocks, BLOCK)
    cumul = jnp.cumsum(fading_exponent.reshape(blocks, BLOCK), axis=-1)
    causal = jnp.tril(jnp.ones((BLOCK, BLOCK), bool))
    strict = jnp.tril(jnp.ones((BLOCK, BLOCK), bool), -1)
    gaps_log = cumul[:, :, None] - cumul[:, None, :]
    within = jnp.where(causal, jnp.exp(jnp.where(causal, gaps_log, 0.0)), 0.0)
    keys_beta = key_blocks * beta_blocks[..., None]
    strict_part = jnp.where(
        strict, jnp.einsum("nid,njd->nij", keys_beta, key_blocks, precision=highest) * within, 0.0
    )
    targets = jnp.concatenate(
        [value_blocks * beta_blocks[..., None], keys_beta * jnp.exp(cumul)[..., None]], axis=-1
    )
    system = jnp.eye(BLOCK, dtype=jnp.float32) + strict_part
    solved = lax.linalg.triangular_solve(system, targets, left_side=True, lower=True)
    width_v = value_blocks.shape[-1]
    width_k = key_blocks.shape[-1]
    pseudo_values = solved[..., :width_v]
    decayed_keys = solved[..., width_v:]
    carried_values = jnp.concatenate(
        [jnp.zeros((blocks, BLOCK, width_k), jnp.float32), pseudo_values], axis=-1
    )
    trailing = key_blocks * jnp.exp(cumul[:, -1:] - cumul)[..., None]
    block_decay = jnp.exp(cumul[:, -1])

    def advance(memory, inputs):
        pseudo, decayed, trail_keys, shrink = inputs
        fresh_values = pseudo - jnp.dot(decayed, memory, precision=highest)
        memory = memory * shrink + jnp.dot(trail_keys.T, fresh_values, precision=highest)
        return (memory, None)

    start_map = jnp.concatenate(
        [jnp.eye(width_k, dtype=jnp.float32), jnp.zeros((width_k, width_v), jnp.float32)], axis=1
    )
    memory, _ = lax.scan(advance, start_map, (carried_values, decayed_keys, trailing, block_decay))
    return memory


def combine_maps(earlier, later):
    return (compose(later[0], earlier[0]), compose(later[0], earlier[1]) + later[1])


def body(
    context_activations,
    first_generated_activation,
    address_projection,
    payload_projection,
    lookup_projection,
    exit_gating_projection,
    writing_intensity_projection,
    fading_projection,
    channel_fading_speed,
    extra_fading_log,
    readout_normalizer_gain,
    exit_projection,
):
    head_size = readout_normalizer_gain.shape[0]
    current_heads = address_projection.shape[1] // head_size
    first_head = lax.axis_index("tp") * current_heads
    beta_cols = lax.dynamic_slice_in_dim(writing_intensity_projection, first_head, current_heads, 1)
    decay_cols = lax.dynamic_slice_in_dim(fading_projection, first_head, current_heads, 1)
    logit_weight = jnp.concatenate([beta_cols, decay_cols], axis=1)
    fading_speeds = lax.dynamic_slice_in_dim(channel_fading_speed, first_head, current_heads, 0)
    seq_count, length = (context_activations.shape[0], context_activations.shape[1])
    portion = lax.all_gather(context_activations, "tp", axis=2, tiled=True)
    key_sum = jnp.einsum(
        "abf,fc->abc", portion, address_projection, preferred_element_type=jnp.float32
    )
    value_sum = jnp.einsum(
        "abf,fc->abc", portion, payload_projection, preferred_element_type=jnp.float32
    )
    logit_sum = jnp.einsum("abf,fc->abc", portion, logit_weight, preferred_element_type=jnp.float32)
    shaped = (seq_count, length, current_heads, head_size)
    keys_here = unit_rows(jax.nn.silu(key_sum).reshape(shaped)).astype(jnp.bfloat16)
    values_here = jax.nn.silu(value_sum).reshape(shaped).astype(jnp.bfloat16)
    current_scores = logit_sum.astype(jnp.bfloat16)
    beta_gate = jax.nn.sigmoid(current_scores[..., :current_heads].astype(jnp.float32))
    fading_exponent = extra_fading_log - fading_speeds * jax.nn.softplus(
        current_scores[..., current_heads:].astype(jnp.float32)
    )
    maps = jax.vmap(jax.vmap(segment_map, in_axes=(1, 1, 1, 1)))(
        keys_here.astype(jnp.float32), values_here.astype(jnp.float32), beta_gate, fading_exponent
    )
    own_moves = maps[..., :head_size]
    own_offset = maps[..., head_size:]
    heads_shape = (seq_count, current_heads, head_size)
    new_keys = unit_rows(
        jax.nn.silu(
            jnp.dot(
                first_generated_activation, address_projection, preferred_element_type=jnp.float32
            )
        ).reshape(heads_shape)
    )
    new_values = jax.nn.silu(
        jnp.dot(first_generated_activation, payload_projection, preferred_element_type=jnp.float32)
    ).reshape(heads_shape)
    new_queries = unit_rows(
        jax.nn.silu(
            jnp.dot(
                first_generated_activation, lookup_projection, preferred_element_type=jnp.float32
            )
        ).reshape(heads_shape)
    )
    out_gate = jax.nn.silu(
        jnp.dot(
            first_generated_activation, exit_gating_projection, preferred_element_type=jnp.float32
        )
    ).reshape(heads_shape)
    new_logits = jnp.dot(
        first_generated_activation, logit_weight, preferred_element_type=jnp.float32
    )
    new_beta = jax.nn.sigmoid(new_logits[:, :current_heads])
    new_decay = jnp.exp(-fading_speeds * jax.nn.softplus(new_logits[:, current_heads:]))
    intersection_kq = jnp.sum(new_keys * new_queries, axis=-1, keepdims=True)
    carried_query = new_decay[..., None] * (
        new_queries - new_beta[..., None] * new_keys * intersection_kq
    )
    own_write = new_beta[..., None] * new_values * intersection_kq
    identity = jnp.broadcast_to(jnp.eye(head_size, dtype=jnp.float32), own_moves.shape)
    prefix_moves, prefix_offset = carried_in(
        (own_moves, own_offset), "sp", combine_maps, (identity, jnp.zeros_like(own_offset))
    )
    states_here = compose(own_moves, prefix_offset) + own_offset

    def chain_later(earlier, later):
        return compose(earlier, later)

    later_moves = carried_in_2(own_moves, "sp", chain_later, identity)
    lifted = jnp.einsum("shjk,shj->shk", later_moves, carried_query, precision=highest)
    term = jnp.einsum("shk,shkv->shv", lifted, own_offset, precision=highest)
    read = lax.psum(term, "sp") + own_write
    state_cache = states_here.astype(jnp.bfloat16)[:, None]
    normed = (
        read
        * lax.rsqrt(jnp.mean(read * read, axis=-1, keepdims=True) + norm_eps)
        * readout_normalizer_gain
        * out_gate
    )
    normed = normed.astype(jnp.bfloat16).reshape(seq_count, current_heads * head_size)
    partial_out = jnp.dot(normed, exit_projection, preferred_element_type=jnp.float32)
    step_out = lax.psum_scatter(partial_out, "tp", scatter_dimension=1, tiled=True).astype(
        jnp.bfloat16
    )
    return (state_cache, step_out)


def solution(mesh):
    placed = (
        P(None, "sp", "tp"),
        P(),
        P(None, "tp"),
        P(None, "tp"),
        P(None, "tp"),
        P(None, "tp"),
        P(),
        P(),
        P(),
        P(None, "sp", "tp"),
        P(),
        P("tp", None),
    )
    return jax.shard_map(
        body,
        mesh=mesh,
        in_specs=placed,
        out_specs=(P(None, "sp", "tp", None, None), P(None, "tp")),
        check_vma=False,
    )
```

profile of v0, /device:TPU:0, one launch (start us, length us, event | category | flops | bytes accessed | tf_op | source)
XLA Modules:
  0.0 188.7 jit_solution(4630512967896987474)
XLA Ops:
  7.2 0.7 all-gather.5.cloned.1.call-update
  8.1 1.3 dynamic_slice.48
  10.2 1.6 multiply_reduce_fusion.4
  11.8 1.1 multiply_reduce_fusion.3
  13.1 0.9 constant_dynamic-slice_fusion.1
  14.0 0.9 convolution_bitcast_fusion.6
  15.1 34.9 %all-gather.5.cloned.1.call-done = bf16[2,256,4096]{2,1,0:T(8,128)(2,1)} async-done(((bf16[2,256,512]{2,1,0:T(8,128)(2,1)}), bf16[2,256,4096]{2,1,0:T(8,128)(2,1)}) %all-gather.5.cloned.1.call-update) | async-done | bytes 4194320 | tf_op jit(solution)/shard_map/all_gather | solution.py:124
  50.0 3.4 %fusion.31 = bf16[2,256,2]{1,2,0:T(2,128)(2,1)S(1)} fusion(bf16[2,256,4096]{2,1,0:T(8,128)(2,1)} %all-gather.5.cloned.1.call-done, bf16[4096,1]{0,1:T(2,128)(2,1)S(1)} %get-tuple-element.365, bf16[4096,1]{0,1:T(2,128)(2,1)S(1)} %get-tuple-element.366), kind=kOutput, calls=%fused_computation.41 | convolution fusion | flops 8422400 | bytes 4212736 | tf_op jit(solution)/shard_map/abf,fc->abc/dot_general | solution.py:131
  53.3 0.7 fusion.63
  54.2 0.5 reduce_window_sum.11
  55.0 3.6 %multiply_reduce_fusion = (f32[2,256]{1,0:T(2,128)S(1)}, f32[2,256,128]{2,1,0:T(8,128)S(1)}) fusion(bf16[2,256,4096]{2,1,0:T(8,128)(2,1)} %all-gather.5.cloned.1.call-done, bf16[4096,128]{1,0:T(8,128)(2,1)S(1)} %copy-done), kind=kOutput, calls=%fused_computation.60 | convolution fusion | flops 537263616 | bytes 5507072 | tf_op jit(solution)/shard_map/abf,fc->abc/dot_general | solution.py:125
  58.7 0.4 fusion.27
  59.1 39.3 %custom-call.3 = f32[2,1,4,1,64,64]{4,5,3,2,1,0:T(8,128)S(1)} custom-call(f32[2,1,4,1,64,64]{5,4,3,2,1,0:T(8,128)S(1)} %fusion.27), custom_call_target="InvertDiagBlocksLowerTriangular" | custom-call | tf_op jit(solution)/shard_map/vmap(vmap())/triangular_solve | solution.py:74
  98.5 3.5 %multiply_convert_fusion = bf16[2,256,128]{2,1,0:T(8,128)(2,1)S(1)} fusion(bf16[2,256,4096]{2,1,0:T(8,128)(2,1)} %all-gather.5.cloned.1.call-done, bf16[4096,128]{1,0:T(8,128)(2,1)S(1)} %copy-done.5), kind=kOutput, calls=%fused_computation.56 | convolution fusion | flops 537198592 | bytes 5373952 | tf_op jit(solution)/shard_map/abf,fc->abc/dot_general | solution.py:128
  102.2 0.7 convolution_bitcast_fusion.3
  103.1 3.0 %while.39 = (s32[]{:T(128)}, f32[2,1,128,256]{3,2,0,1:T(8,128)S(1)}, f32[4,2,1]{1,2,0:T(1,128)S(1)}, f32[4,2,1,64,128]{4,3,0,1,2:T(8,128)S(1)}, f32[4,2,1,64,256...) while((s32[]{:T(128)}, f32[2,1,128,256]{3,2,0,1:T(8,128)S(1)}, ...), condition=%wide.region_3.4_spmd, body=%wide.region_2.3_spmd.sunk | while | flops 100827136 | bytes 1312357 | solution.py:94
  103.4 0.4 fusion.110
  104.1 0.4 fusion.110
  104.9 0.4 fusion.110
  105.6 0.4 fusion.110
  106.2 16.2 %all-gather.2 = f32[8,1,128,128]{3,2,1,0:T(8,128)S(1)} all-gather(f32[2,1,128,128]{3,2,1,0:T(8,128)S(1)} %slice_bitcast_fusion.1), channel_id=4, replica_groups=mesh['sp'=4,'tp'=8] {'sp'}, dimensions={0}, use_global_device_ids=true | all-gather | bytes 655360 | tf_op jit(solution)/shard_map/all_gather | solution.py:36
  122.4 1.8 while.40
  122.4 0.4 fusion.113
  124.7 12.1 %psum.7 = f32[2,1,128]{2,0,1:T(2,128)S(1)} all-reduce(f32[2,1,128]{2,0,1:T(2,128)S(1)} %bitcast.222), channel_id=1, replica_groups=mesh['sp'=4,'tp'=8] {'sp'}, use_global_device_ids=true, to_apply=%region_11.12 | all-reduce | flops 256 | bytes 2048 | tf_op jit(solution)/shard_map/psum | solution.py:190
  136.8 1.6 multiply_reduce_fusion.1
  138.5 3.3 %convolution_bitcast_fusion.2 = f32[4096,2]{1,0:T(8,128)} fusion(bf16[128,4096]{1,0:T(8,128)(2,1)S(1)} %copy-done.1, f32[2,1,128]{2,0,1:T(2,128)S(1)} %get-tuple-element.345, f32[128]{0:T(128)S(1)} %copy-done.4, f32[2]{0:T(128)S(1)} %add_rsqrt_fusion.1, bf16[2,4096]{1,0:T(2,128)(2,1)S(1)} %copy-done.2, bf16[4096,128]{1,0:T(8,128)(2,1)} %param.23), kind=kOutput, calls=%fused_computation.29 | convolution fusion | flops 4196352 | bytes 2147848
  141.8 14.4 %all-gather = bf16[8,1,128,128]{3,2,1,0:T(8,128)(2,1)S(1)} all-gather(bf16[2,1,128,128]{3,2,1,0:T(8,128)(2,1)S(1)} %get-tuple-element.355), channel_id=2, replica_groups=mesh['sp'=4,'tp'=8] {'sp'}, dimensions={0}, use_global_device_ids=true | all-gather | bytes 327680 | tf_op jit(solution)/shard_map/all_gather | solution.py:14
  156.2 13.8 %all-gather.1 = bf16[8,1,128,128]{3,2,1,0:T(8,128)(2,1)S(1)} all-gather(bf16[2,1,128,128]{3,2,1,0:T(8,128)(2,1)S(1)} %get-tuple-element.354), channel_id=3, replica_groups=mesh['sp'=4,'tp'=8] {'sp'}, dimensions={0}, use_global_device_ids=true | all-gather | bytes 327680 | tf_op jit(solution)/shard_map/all_gather | solution.py:14
  170.0 1.1 while.41
  171.1 0.9 fusion.30
  172.0 8.3 %reduce-scatter.4.cloned.1.call-done = f32[512,2]{1,0:T(8,128)} async-done(((f32[4096,2]{1,0:T(8,128)}), f32[512,2]{1,0:T(8,128)}) %reduce-scatter.4.cloned.1.call-update) | async-done | bytes 4112
  180.3 1.6 copy.60
  (66 shorter events, 5.5 us)
Async XLA Ops:
  7.2 4.6 %copy-start = (bf16[4096,128]{1,0:T(8,128)(2,1)S(1)}, bf16[4096,128]{1,0:T(8,128)(2,1)}, u32[]{:S(2)}) copy-start(bf16[4096,128]{1,0:T(8,128)(2,1)} %param.20) | copy-start | bytes 3145732
  7.2 46.2 %copy-start.3 = (f32[2,256,1]{1,2,0:T(1,128)S(1)}, f32[2,256,1]{1,2,0:T(1,128)}, u32[]{:S(2)}) copy-start(f32[2,256,1]{1,2,0:T(1,128)} %param.27) | copy-start | bytes 6148
  7.2 42.8 %all-gather.5.cloned.1.call-start = ((), (), s32[]{:S(2)}) async-start(), calls=%async_computation.1 | async-start | bytes 4718592 | tf_op jit(solution)/shard_map/all_gather | solution.py:124
  7.9 172.3 %reduce-scatter.4.cloned.1.call-start = ((), (), s32[]{:S(2)}) async-start(), calls=%async_computation.2 | async-start | bytes 2359296
  54.1 44.4 %copy-start.5 = (bf16[4096,128]{1,0:T(8,128)(2,1)S(1)}, bf16[4096,128]{1,0:T(8,128)(2,1)}, u32[]{:S(2)}) copy-start(bf16[4096,128]{1,0:T(8,128)(2,1)} %param.21) | copy-start | bytes 3145732
  106.1 30.8 %copy-start.2 = (bf16[2,4096]{1,0:T(2,128)(2,1)S(1)}, bf16[2,4096]{1,0:T(2,128)(2,1)}, u32[]{:S(2)}) copy-start(bf16[2,4096]{1,0:T(2,128)(2,1)} %param.19) | copy-start | bytes 49156
  106.1 32.4 %copy-start.1 = (bf16[128,4096]{1,0:T(8,128)(2,1)S(1)}, bf16[128,4096]{1,0:T(8,128)(2,1)}, u32[]{:S(2)}) copy-start(bf16[128,4096]{1,0:T(8,128)(2,1)} %param.29) | copy-start | bytes 3145732
  106.1 32.4 %copy-start.4 = (f32[128]{0:T(128)S(1)}, f32[128]{0:T(128)}, u32[]{:S(2)}) copy-start(f32[128]{0:T(128)} %param.28) | copy-start | bytes 1540
Sparse Core Ops, SparseCore 0:
  9.9 40.0 all-gather.4
  141.9 38.3 reduce-scatter.3
where the time goes:
time: 189 us
  blocking collectives  56.6 us (30%)
  waiting for transfers between devices  43.9 us (23%)
  other arithmetic  41.5 us (22%)
  matrix products  26.6 us (14%)
  between operations  15 us (8%)
  local copies, waits for them, and re-layouts  4.71 us (2%)
    another operation x1, other arithmetic, segment_map(): lax.linalg.triangular_solve(system, targets, left_side=True, lower=True)  39.3 us
    all_gather x1, waiting for transfers between devices, body(): portion = lax.all_gather(context_activations, 'tp', axis=2, tiled=True)  34.9 us
    all_gather x2, blocking collectives, carried_in(): lax.all_gather(part.astype(kind), axis)  28.2 us
    all_gather x1, blocking collectives, carried_in_2(): everything = lax.all_gather(value, axis)  16.2 us
    psum x1, blocking collectives, body(): read = lax.psum(term, 'sp') + own_write  12.1 us
    unnamed x3, waiting for transfers between devices  8.97 us
  transfers between devices with their start and end apart: 2, of which 2 were waited for; matrix products, arithmetic and copies ran while one was open for 4% of the time, Pallas kernels for 0%

commit v1 on v0

--- a/solution.py
+++ b/solution.py
@@ -6,6 +6,17 @@
 BLOCK = 64
 norm_eps = 1e-06
 highest = lax.Precision.HIGHEST
+
+
+def around_the_ring(x, mesh_axis, dim):
+    devices = lax.axis_size(mesh_axis)
+    right = [(i, (i + 1) % devices) for i in range(devices)]
+    terms = [x]
+    for stride in range(1, devices):
+        terms = [lax.ppermute(terms[0], mesh_axis, right), *terms]
+    result = jnp.concatenate(terms, axis=dim)
+    offset = (lax.axis_index(mesh_axis) + 1) * terms[-1].shape[dim]
+    return jnp.roll(result, offset, axis=dim)
 
 
 def carried_in(value, axis, combine, identity):
@@ -121,7 +132,7 @@
     logit_weight = jnp.concatenate([beta_cols, decay_cols], axis=1)
     fading_speeds = lax.dynamic_slice_in_dim(channel_fading_speed, first_head, current_heads, 0)
     seq_count, length = (context_activations.shape[0], context_activations.shape[1])
-    portion = lax.all_gather(context_activations, "tp", axis=2, tiled=True)
+    portion = around_the_ring(context_activations, "tp", 2)
     key_sum = jnp.einsum(
         "abf,fc->abc", portion, address_projection, preferred_element_type=jnp.float32
     )

time: 189 us -> 222 us (1.17)
  waiting for transfers between devices: 43.9 us -> 67.6 us
  local copies, waits for them, and re-layouts: 4.71 us -> 16.4 us
  matrix products: 26.6 us -> 23.1 us
    ppermute x0 -> x7, waiting for transfers between devices: none -> 59 us  [around_the_ring(): terms = [lax.ppermute(terms[0], mesh_axis, right), *terms]]
    all_gather x1 -> x0, waiting for transfers between devices: 34.9 us -> none  [body(): portion = lax.all_gather(context_activations, 'tp', axis=2, tiled=True)]
    unnamed x14 -> x35, local copies, waits for them, and re-layouts: 1.78 us -> 6.7 us
    mul x4, local copies, waits for them, and re-layouts: 0.04 us -> 2.65 us  [advance(): memory * shrink + jnp.dot(trail_keys.T, fresh_values, precision=highest)]
    unnamed x3 -> x2, waiting for transfers between devices: 8.97 us -> 8.52 us
  transfers between devices with their start and end apart: 2 -> 8, of which waited for: 2 -> 8; matrix products, arithmetic and copies ran while one was open for 4% -> 4% of each run, Pallas kernels for 0% -> 0%
where the time goes in v1:
time: 222 us; the launch traced here: 221 us
  waiting for transfers between devices  67.6 us (30%)
  blocking collectives  55.8 us (25%)
  other arithmetic  42 us (19%)
  matrix products  23.1 us (10%)
  local copies, waits for them, and re-layouts  16.4 us (7%)
  between operations  15.1 us (7%)
    ppermute x7, waiting for transfers between devices, around_the_ring(): terms = [lax.ppermute(terms[0], mesh_axis, right), *terms]  59 us
    another operation x1, other arithmetic, segment_map(): lax.linalg.triangular_solve(system, targets, left_side=True, lower=True)  39.3 us
    all_gather x2, blocking collectives, carried_in(): lax.all_gather(part.astype(kind), axis)  28.1 us
    all_gather x1, blocking collectives, carried_in_2(): everything = lax.all_gather(value, axis)  15.8 us
    psum x1, blocking collectives, body(): read = lax.psum(term, 'sp') + own_write  11.8 us
    unnamed x2, waiting for transfers between devices  8.52 us
    unnamed x35, local copies, waits for them, and re-layouts  6.7 us
  transfers between devices with their start and end apart: 8, of which 8 were waited for; matrix products, arithmetic and copies ran while one was open for 4% of the time, Pallas kernels for 0%

profile of v1, /device:TPU:0, one launch (start us, length us, event | category | flops | bytes accessed | tf_op | source)
XLA Modules:
  0.0 221.0 jit_solution(9877608382965338271)
XLA Ops:
  7.8 9.9 %collective-permute-done = bf16[2,256,512]{2,1,0:T(8,128)(2,1)S(1)} collective-permute-done((bf16[2,256,512]{2,1,0:T(8,128)(2,1)}, bf16[2,256,512]{2,1,0:T(8,128)(2,1)S(1)}, u32[]{:S(2)}, u32[]{:S(2)}) %collective-permute-start) | collective-permute-done | bytes 524320 | tf_op jit(solution)/shard_map/ppermute | solution.py:16
  17.7 9.5 %collective-permute-done.1 = bf16[2,256,512]{2,1,0:T(8,128)(2,1)S(1)} collective-permute-done((bf16[2,256,512]{2,1,0:T(8,128)(2,1)S(1)}, bf16[2,256,512]{2,1,0:T(8,128)(2,1)S(1)}, u32[]{:S(2)}, u32[]{:S(2)}) %collective-permute-start.1) | collective-permute-done | bytes 524320 | tf_op jit(solution)/shard_map/ppermute | solution.py:16
  27.2 1.6 multiply_reduce_fusion.4
  28.8 7.9 %collective-permute-done.2 = bf16[2,256,512]{2,1,0:T(8,128)(2,1)S(1)} collective-permute-done((bf16[2,256,512]{2,1,0:T(8,128)(2,1)S(1)}, bf16[2,256,512]{2,1,0:T(8,128)(2,1)S(1)}, u32[]{:S(2)}, u32[]{:S(2)}) %collective-permute-start.2) | collective-permute-done | bytes 524320 | tf_op jit(solution)/shard_map/ppermute | solution.py:16
  36.9 1.2 dynamic_slice.52
  39.5 1.1 multiply_reduce_fusion.3
  40.6 5.8 %collective-permute-done.3 = bf16[2,256,512]{2,1,0:T(8,128)(2,1)} collective-permute-done((bf16[2,256,512]{2,1,0:T(8,128)(2,1)S(1)}, bf16[2,256,512]{2,1,0:T(8,128)(2,1)}, u32[]{:S(2)}, u32[]{:S(2)}) %collective-permute-start.3) | collective-permute-done | bytes 524320 | tf_op jit(solution)/shard_map/ppermute | solution.py:16
  46.5 0.9 constant_dynamic-slice_fusion.1
  47.5 8.6 %collective-permute-done.4 = bf16[2,256,512]{2,1,0:T(8,128)(2,1)S(1)} collective-permute-done((bf16[2,256,512]{2,1,0:T(8,128)(2,1)}, bf16[2,256,512]{2,1,0:T(8,128)(2,1)S(1)}, u32[]{:S(2)}, u32[]{:S(2)}) %collective-permute-start.4) | collective-permute-done | bytes 524320 | tf_op jit(solution)/shard_map/ppermute | solution.py:16
  57.0 8.6 %collective-permute-done.5 = bf16[2,256,512]{2,1,0:T(8,128)(2,1)S(1)} collective-permute-done((bf16[2,256,512]{2,1,0:T(8,128)(2,1)S(1)}, bf16[2,256,512]{2,1,0:T(8,128)(2,1)S(1)}, u32[]{:S(2)}, u32[]{:S(2)}) %collective-permute-start.5) | collective-permute-done | bytes 524320 | tf_op jit(solution)/shard_map/ppermute | solution.py:16
  66.3 8.7 %collective-permute-done.6 = bf16[2,256,512]{2,1,0:T(8,128)(2,1)S(1)} collective-permute-done((bf16[2,256,512]{2,1,0:T(8,128)(2,1)S(1)}, bf16[2,256,512]{2,1,0:T(8,128)(2,1)S(1)}, u32[]{:S(2)}, u32[]{:S(2)}) %collective-permute-start.6) | collective-permute-done | bytes 524320 | tf_op jit(solution)/shard_map/ppermute | solution.py:16
  75.3 1.1 constant_dynamic-update-slice_fusion.12
  76.9 1.1 constant_dynamic-update-slice_fusion.4
  78.4 1.4 multiply_reduce_fusion
  79.7 1.9 copy-done.1
  81.6 1.2 fusion.37
  85.4 39.3 %custom-call.3 = f32[2,1,4,1,64,64]{4,5,3,2,1,0:T(8,128)S(1)} custom-call(f32[2,1,4,1,64,64]{5,4,3,2,1,0:T(8,128)S(1)} %fusion.33), custom_call_target="InvertDiagBlocksLowerTriangular" | custom-call | tf_op jit(solution)/shard_map/vmap(vmap())/triangular_solve | solution.py:85
  124.8 3.8 %multiply_convert_fusion = bf16[2,256,128]{2,1,0:T(8,128)(2,1)S(1)} fusion(bf16[4096,128]{1,0:T(8,128)(2,1)} %param.21, bf16[2,256,8192]{2,1,0:T(8,128)(2,1)} %copy-done.1, s32[]{:T(128)S(6)} %select_n.97), kind=kOutput, calls=%fused_computation.59 | convolution fusion | flops 537198592 | bytes 5373956 | tf_op jit(solution)/shard_map/abf,fc->abc/dot_general | solution.py:139
  129.6 1.3 copy.42
  131.0 0.9 broadcast_in_dim.25
  131.9 5.6 %while.39 = (s32[]{:T(128)}, f32[2,1,128,256]{3,2,0,1:T(8,128)S(1)}, f32[4,2,1]{1,2,0:T(1,128)}, f32[4,2,1,64,128]{4,3,0,1,2:T(8,128)S(1)}, f32[4,2,1,64,256]{4,...) while((s32[]{:T(128)}, f32[2,1,128,256]{3,2,0,1:T(8,128)S(1)}, f32[4,2,1]{1,2,0:T(1,128)}, ...), condition=%wide.region_3.4_spmd, body=%wide.region_2.3_spmd.sunk | while | flops 100827136 | bytes 1312357 | solution.py:105
  137.5 15.8 %all-gather.2 = f32[8,1,128,128]{3,2,1,0:T(8,128)S(1)} all-gather(f32[2,1,128,128]{3,2,1,0:T(8,128)S(1)} %slice_bitcast_fusion.1), channel_id=4, replica_groups=mesh['sp'=4,'tp'=8] {'sp'}, dimensions={0}, use_global_device_ids=true | all-gather | bytes 655360 | tf_op jit(solution)/shard_map/all_gather | solution.py:47
  154.2 1.8 while.40
  156.0 1.0 convolution_bitcast_fusion.5
  157.2 11.8 %psum.7 = f32[2,1,128]{2,0,1:T(2,128)S(1)} all-reduce(f32[2,1,128]{2,0,1:T(2,128)S(1)} %bitcast.217), channel_id=1, replica_groups=mesh['sp'=4,'tp'=8] {'sp'}, use_global_device_ids=true, to_apply=%region_11.12 | all-reduce | flops 256 | bytes 2048 | tf_op jit(solution)/shard_map/psum | solution.py:201
  169.0 1.6 multiply_reduce_fusion.1
  170.7 3.3 %convolution_bitcast_fusion.2 = f32[4096,2]{1,0:T(8,128)} fusion(bf16[128,4096]{1,0:T(8,128)(2,1)S(1)} %copy-done.3, f32[2,1,128]{2,0,1:T(2,128)S(1)} %get-tuple-element.345, f32[128]{0:T(128)} %param.28, f32[2]{0:T(128)S(1)} %add_rsqrt_fusion.1, bf16[2,4096]{1,0:T(2,128)(2,1)S(1)} %copy-done.5, bf16[4096,128]{1,0:T(8,128)(2,1)} %param.23), kind=kOutput, calls=%fused_computation.29 | convolution fusion | flops 4196352 | bytes 2147848
  173.9 14.3 %all-gather = bf16[8,1,128,128]{3,2,1,0:T(8,128)(2,1)S(1)} all-gather(bf16[2,1,128,128]{3,2,1,0:T(8,128)(2,1)S(1)} %get-tuple-element.355), channel_id=2, replica_groups=mesh['sp'=4,'tp'=8] {'sp'}, dimensions={0}, use_global_device_ids=true | all-gather | bytes 327680 | tf_op jit(solution)/shard_map/all_gather | solution.py:25
  188.2 13.8 %all-gather.1 = bf16[8,1,128,128]{3,2,1,0:T(8,128)(2,1)S(1)} all-gather(bf16[2,1,128,128]{3,2,1,0:T(8,128)(2,1)S(1)} %get-tuple-element.354), channel_id=3, replica_groups=mesh['sp'=4,'tp'=8] {'sp'}, dimensions={0}, use_global_device_ids=true | all-gather | bytes 327680 | tf_op jit(solution)/shard_map/all_gather | solution.py:25
  202.0 1.1 while.41
  204.0 8.5 %reduce-scatter.4.cloned.1.call-done = f32[512,2]{1,0:T(8,128)} async-done(((f32[4096,2]{1,0:T(8,128)}), f32[512,2]{1,0:T(8,128)}) %reduce-scatter.4.cloned.1.call-update) | async-done | bytes 4112
  212.5 1.6 copy.60
  (99 shorter events, 17.9 us)
Async XLA Ops:
  7.2 32.3 %copy-start = (bf16[4096,128]{1,0:T(8,128)(2,1)S(1)}, bf16[4096,128]{1,0:T(8,128)(2,1)}, u32[]{:S(2)}) copy-start(bf16[4096,128]{1,0:T(8,128)(2,1)} %param.20) | copy-start | bytes 3145732
  7.2 69.4 %copy-start.2 = (bf16[2,256,512]{2,1,0:T(8,128)(2,1)S(1)}, bf16[2,256,512]{2,1,0:T(8,128)(2,1)}, u32[]{:S(2)}) copy-start(bf16[2,256,512]{2,1,0:T(8,128)(2,1)} %param.18) | copy-start | bytes 1572868
  7.2 205.3 %reduce-scatter.4.cloned.1.call-start = ((), (), s32[]{:S(2)}) async-start(), calls=%async_computation.1 | async-start | bytes 2359296
  7.2 10.5 %collective-permute-start = (bf16[2,256,512]{2,1,0:T(8,128)(2,1)}, bf16[2,256,512]{2,1,0:T(8,128)(2,1)S(1)}, u32[]{:S(2)}, u32[]{:S(2)}) collective-permute-start(bf16[2,256,512]{2,1,0:T(8,128)(2,1)} %param.18), channel_id=1, source_target_pairs={{0,1},{1,2},{2,3},{3,4},{4,5},{5,6},{6,7},{7,0},{8,9},{9,10},{10,1... | collective-permute-start | bytes 1572872 | tf_op jit(solution)/shard_map/ppermute | solution.py:16
  17.7 9.5 %collective-permute-start.1 = (bf16[2,256,512]{2,1,0:T(8,128)(2,1)S(1)}, bf16[2,256,512]{2,1,0:T(8,128)(2,1)S(1)}, u32[]{:S(2)}, u32[]{:S(2)}) collective-permute-start(bf16[2,256,512]{2,1,0:T(8,128)(2,1)S(1)} %collective-permute-done), channel_id=1, source_target_pairs={{0,1},{1,2},{2,3},{3,4},{4,5},{5,6},{6,7},{7,0},{8,9},{9,10},{10,1... | collective-permute-start | bytes 1572872 | tf_op jit(solution)/shard_map/ppermute | solution.py:16
  27.2 9.5 %collective-permute-start.2 = (bf16[2,256,512]{2,1,0:T(8,128)(2,1)S(1)}, bf16[2,256,512]{2,1,0:T(8,128)(2,1)S(1)}, u32[]{:S(2)}, u32[]{:S(2)}) collective-permute-start(bf16[2,256,512]{2,1,0:T(8,128)(2,1)S(1)} %collective-permute-done.1), channel_id=1, source_target_pairs={{0,1},{1,2},{2,3},{3,4},{4,5},{5,6},{6,7},{7,0},{8,9},{9,10},{10,1... | collective-permute-start | bytes 1572872 | tf_op jit(solution)/shard_map/ppermute | solution.py:16
  36.7 9.6 %collective-permute-start.3 = (bf16[2,256,512]{2,1,0:T(8,128)(2,1)S(1)}, bf16[2,256,512]{2,1,0:T(8,128)(2,1)}, u32[]{:S(2)}, u32[]{:S(2)}) collective-permute-start(bf16[2,256,512]{2,1,0:T(8,128)(2,1)S(1)} %collective-permute-done.2), channel_id=1, source_target_pairs={{0,1},{1,2},{2,3},{3,4},{4,5},{5,6},{6,7},{7,0},{8,9},{9,10},{10,1... | collective-permute-start | bytes 1572872 | tf_op jit(solution)/shard_map/ppermute | solution.py:16
  36.8 41.5 %copy-start.4 = (f32[128,128]{0,1:T(8,128)}, f32[128,128]{0,1:T(8,128)S(1)}, u32[]{:S(2)}) copy-start(f32[128,128]{0,1:T(8,128)S(1)} %fusion.64) | copy-start | bytes 196612
  46.3 9.7 %collective-permute-start.4 = (bf16[2,256,512]{2,1,0:T(8,128)(2,1)}, bf16[2,256,512]{2,1,0:T(8,128)(2,1)S(1)}, u32[]{:S(2)}, u32[]{:S(2)}) collective-permute-start(bf16[2,256,512]{2,1,0:T(8,128)(2,1)} %collective-permute-done.3), channel_id=1, source_target_pairs={{0,1},{1,2},{2,3},{3,4},{4,5},{5,6},{6,7},{7,0},{8,9},{9,10},{10,1... | collective-permute-start | bytes 1572872 | tf_op jit(solution)/shard_map/ppermute | solution.py:16
  46.5 19.0 %copy-start.7 = (f32[2]{0:T(128)}, f32[2]{0:T(128)S(1)}, u32[]{:S(2)}) copy-start(f32[2]{0:T(128)S(1)} %multiply_reduce_fusion.2) | copy-start | bytes 28
  56.1 9.5 %collective-permute-start.5 = (bf16[2,256,512]{2,1,0:T(8,128)(2,1)S(1)}, bf16[2,256,512]{2,1,0:T(8,128)(2,1)S(1)}, u32[]{:S(2)}, u32[]{:S(2)}) collective-permute-start(bf16[2,256,512]{2,1,0:T(8,128)(2,1)S(1)} %collective-permute-done.4), channel_id=1, source_target_pairs={{0,1},{1,2},{2,3},{3,4},{4,5},{5,6},{6,7},{7,0},{8,9},{9,10},{10,1... | collective-permute-start | bytes 1572872 | tf_op jit(solution)/shard_map/ppermute | solution.py:16
  57.0 8.6 %copy-start.8 = (f32[2]{0:T(128)}, f32[2]{0:T(128)S(1)}, u32[]{:S(2)}) copy-start(f32[2]{0:T(128)S(1)} %get-tuple-element.362) | copy-start | bytes 28
  65.6 9.5 %collective-permute-start.6 = (bf16[2,256,512]{2,1,0:T(8,128)(2,1)S(1)}, bf16[2,256,512]{2,1,0:T(8,128)(2,1)S(1)}, u32[]{:S(2)}, u32[]{:S(2)}) collective-permute-start(bf16[2,256,512]{2,1,0:T(8,128)(2,1)S(1)} %collective-permute-done.5), channel_id=1, source_target_pairs={{0,1},{1,2},{2,3},{3,4},{4,5},{5,6},{6,7},{7,0},{8,9},{9,10},{10,1... | collective-permute-start | bytes 1572872 | tf_op jit(solution)/shard_map/ppermute | solution.py:16
  76.8 5.9 %copy-start.6 = (f32[2,256,1]{1,2,0:T(1,128)S(1)}, f32[2,256,1]{1,2,0:T(1,128)}, u32[]{:S(2)}) copy-start(f32[2,256,1]{1,2,0:T(1,128)} %param.27) | copy-start | bytes 6148
  78.3 3.2 %copy-start.1 = (bf16[2,256,8192]{2,1,0:T(8,128)(2,1)}, bf16[2,256,8192]{2,1,0:T(8,128)(2,1)S(1)}, u32[]{:S(2)}) copy-start(bf16[2,256,8192]{2,1,0:T(8,128)(2,1)S(1)} %constant_dynamic-update-slice_fusion) | copy-start | bytes 25165828
  128.6 40.4 %copy-start.5 = (bf16[2,4096]{1,0:T(2,128)(2,1)S(1)}, bf16[2,4096]{1,0:T(2,128)(2,1)}, u32[]{:S(2)}) copy-start(bf16[2,4096]{1,0:T(2,128)(2,1)} %param.19) | copy-start | bytes 49156
  128.9 41.8 %copy-start.3 = (bf16[128,4096]{1,0:T(8,128)(2,1)S(1)}, bf16[128,4096]{1,0:T(8,128)(2,1)}, u32[]{:S(2)}) copy-start(bf16[128,4096]{1,0:T(8,128)(2,1)} %param.29) | copy-start | bytes 3145732
Sparse Core Ops, SparseCore 0:
  174.1 38.3 reduce-scatter.3
